TPU v7x, 32 devices: a whole 2x2x4 slice. The times are simulated.
32 devices in a mesh: sp: 16 (over z, y, core), tp: 2 (over x).
Axes of the slice: x: 2, y: 2, z: 4, core: 2. Of those that a mesh axis runs over, the one named last changes fastest.
Arguments:
- tokens: bfloat16 [4096, 2048], P('sp'), may hold values from -28 to 28
- query_weight: bfloat16 [2048, 1536], P(None, 'tp'), may hold values from -0.125 to 0.125
- key_weight: bfloat16 [2048, 1536], P(None, 'tp'), may hold values from -0.125 to 0.125
- value_weight: bfloat16 [2048, 1536], P(None, 'tp'), may hold values from -0.125 to 0.125
- out_weight: bfloat16 [512, 2048], P(None, 'tp'), may hold values from -1 to 1
Outputs:
- mixed: bfloat16 [4096, 2048], P('sp', 'tp')
- total_log: float32 [4, 4096], P('tp', 'sp')
All inputs are finite; a program needn't handle non-finite values.
Results may differ from a plain program's by a relative error of at most 0.012.
The roundings to bfloat16 on the way count: a program that leaves them out, or rounds other values in their place, can miss the bound.
Values may be sent and summed in bfloat16 or wider, within the bound.
A program may use at most 64 MiB of HBM per device.

v0:
```python
import functools
import jax
import jax.numpy as jnp
from jax import lax
from jax.experimental import pallas as pl
from jax.experimental.pallas import tpu as pltpu
from jax.sharding import PartitionSpec as P

HEADS = 4
HEAD_DIM = 128
NEAR_WINDOW = 128
MIDDLE_WINDOW = 512
MIDDLE_DILATION = 4
FAR_WINDOW = 2048
FAR_DILATION = 16


def from_behind(block, axis, distance):
    devices = range(lax.axis_size(axis))
    route = [(i - distance, i) for i in devices if i - distance in devices]
    return lax.ppermute(block, axis, route)


def window_table():
    return ((NEAR_WINDOW, 1), (MIDDLE_WINDOW, MIDDLE_DILATION), (FAR_WINDOW, FAR_DILATION))


def tail_counts(row_count, distance, held_rows):
    counts = []
    for entry, available in zip(window_table(), held_rows):
        counts.append(max(0, min(available, entry[0] - (distance - 1) * row_count)))
    return counts


def pack_tails(sources, counts):
    selected = [
        source[:, source.shape[1] - amount :]
        for source, amount in zip(sources, counts)
        if amount > 0
    ]
    return jnp.concatenate(selected, axis=1)


def unpack_rows(packed, counts):
    result = []
    cursor = 0
    for amount in counts:
        result.append(packed[:, cursor : cursor + amount])
        cursor = cursor + amount
    return result


def attend_group(group_queries, buffer, window, dilation, first_key, slopes_here):
    row_count = group_queries.shape[0]
    head_count = group_queries.shape[1]
    head_size = group_queries.shape[2]
    query_split = group_queries.reshape(row_count // dilation, dilation, head_count, head_size)
    key_split = buffer[0].reshape(-1, dilation, head_count, head_size)
    value_split = buffer[1].reshape(-1, dilation, head_count, head_size)
    scores = jnp.einsum(
        "mrhe,nrhe->rhmn", query_split, key_split, preferred_element_type=jnp.float32
    ) * head_size ** (-0.5)
    grid_shape = (row_count // dilation, key_split.shape[0])
    query_slot = lax.broadcasted_iota(jnp.int32, grid_shape, 0)
    key_slot = lax.broadcasted_iota(jnp.int32, grid_shape, 1)
    spacing = query_slot + window // dilation - key_slot
    residue = lax.broadcasted_iota(jnp.int32, (dilation, 1, 1), 0)
    key_place = first_key + residue + dilation * key_slot[None]
    valid = (spacing[None] >= 0) & (spacing[None] <= window // dilation) & (key_place >= 0)
    scores = (
        scores
        - slopes_here[None, :, None, None] * (dilation * spacing).astype(jnp.float32)[None, None]
    )
    masked = jnp.where(valid[:, None], scores, -jnp.inf)
    highest = jnp.max(masked, axis=-1, keepdims=True)
    log_sum = highest + jnp.log(jnp.sum(jnp.exp(masked - highest), axis=-1, keepdims=True))
    probs = jnp.exp(masked - log_sum).astype(jnp.bfloat16)
    attended = jnp.einsum("rhmn,nrhe->mrhe", probs, value_split, preferred_element_type=jnp.float32)
    attended = attended.reshape(row_count, head_count, head_size)
    log_rows = jnp.transpose(log_sum[..., 0], (1, 2, 0)).reshape(head_count, row_count)
    return (attended, log_rows)


def local(tokens, query_weight, key_weight, value_weight, out_weight):
    rows_here = tokens.shape[0]
    local_heads = query_weight.shape[1] // (3 * HEAD_DIM)

    def project(weight_matrix):
        product = jnp.dot(tokens, weight_matrix, preferred_element_type=jnp.float32)
        return product.astype(jnp.bfloat16).reshape(rows_here, local_heads, 3, HEAD_DIM)

    queries = project(query_weight)
    keys_all = project(key_weight)
    values_all = project(value_weight)
    table = window_table()
    own = [jnp.stack((keys_all[:, :, index], values_all[:, :, index])) for index in range(3)]
    held = list(own)
    span_now = 1
    while span_now * rows_here < FAR_WINDOW + rows_here:
        counts = tail_counts(rows_here, span_now, [item.shape[1] for item in held])
        packed = pack_tails(held, counts)
        arrived = from_behind(packed, "sp", span_now)
        pieces_in = unpack_rows(arrived, counts)
        for index in range(3):
            if counts[index] > 0:
                joined = jnp.concatenate((pieces_in[index], held[index]), axis=1)
                held[index] = joined
        span_now = span_now * 2
    priors = [held[index][:, : table[index][0]] for index in range(3)]
    position_start = lax.axis_index("sp") * rows_here
    head_ids = (
        lax.axis_index("tp") * local_heads + jnp.arange(local_heads, dtype=jnp.int32)
    ).astype(jnp.float32)
    outputs = []
    logs = []
    for index, (window, dilation) in enumerate(table):
        buffer = jnp.concatenate((priors[index], own[index]), axis=1)
        slopes_here = 2.0 ** (3.0 - 8.0 * (head_ids + 1.0) / HEADS) / window
        attended, log_rows = attend_group(
            queries[:, :, index], buffer, window, dilation, position_start - window, slopes_here
        )
        outputs.append(attended)
        logs.append(log_rows)
    stacked_logs = jnp.stack(logs)
    highest = jnp.max(stacked_logs, axis=0)
    total_log = highest + jnp.log(jnp.sum(jnp.exp(stacked_logs - highest), axis=0))
    mixing = jnp.exp(stacked_logs - total_log)
    merged = outputs[0] * jnp.transpose(mixing[0])[:, :, None]
    merged = merged + outputs[1] * jnp.transpose(mixing[1])[:, :, None]
    merged = merged + outputs[2] * jnp.transpose(mixing[2])[:, :, None]
    merged = merged.astype(jnp.bfloat16).reshape(rows_here, local_heads * HEAD_DIM)
    mixed = jnp.dot(
        lax.all_gather(merged, "tp", axis=1, tiled=True),
        out_weight,
        preferred_element_type=jnp.float32,
    ).astype(jnp.bfloat16)
    return (mixed, total_log)


MESH = pl.DeviceIdType.MESH
MASKED = -1e30


def attend(query, key, value, slope, distance, valid):
    scores = lax.dot_general(
        query, key, (((1,), (1,)), ((), ())), preferred_element_type=jnp.float32
    ) * HEAD_DIM ** (-0.5)
    scores = jnp.where(valid, scores - slope * distance, MASKED)
    highest = jnp.max(scores, axis=-1, keepdims=True)
    weights = jnp.exp(scores - highest)
    total = jnp.sum(weights, axis=-1, keepdims=True)
    probs = (weights * (1.0 / total)).astype(jnp.bfloat16)
    attended = jnp.dot(probs, value, preferred_element_type=jnp.float32)
    return attended, highest + jnp.log(total)


def swap_matrix(rows, width):
    shift = width.bit_length() - 1
    row = lax.broadcasted_iota(jnp.int32, (rows, rows), 0)
    column = lax.broadcasted_iota(jnp.int32, (rows, rows), 1)
    source = ((row & (width - 1)) << shift) + (row >> shift)
    return jnp.where(column == source, 1.0, 0.0).astype(jnp.bfloat16)


def kernel(
    n, n_tp, local_heads,
    tok_hbm, wq_hbm, wk_hbm, wv_hbm,
    both_ref, totals_ref,
    tok, weight, far_send, far_held, back_send, back_held,
    mid_query, mid_own, mid_held, via_held, near_query, near_own, near_held,
    merged_own, merged_held,
    load_sem, far_ssem, far_rsem, back_ssem, back_rsem,
    mid_ssem, mid_rsem, via_ssem, via_rsem, near_ssem, near_rsem, merged_ssem, merged_rsem,
):
    me = lax.axis_index("sp")
    tp = lax.axis_index("tp")
    rows = tok.shape[0]
    width = local_heads * HEAD_DIM
    chunk = rows // n
    peer = 1 - tp

    loads = {}
    tok_load = pltpu.make_async_copy(tok_hbm, tok, load_sem.at[0])
    tok_load.start()
    count = 1
    for group in (2, 1, 0):
        loads[group] = []
        for part, source in enumerate((wq_hbm, wk_hbm, wv_hbm)):
            for head in range(local_heads):
                copy = pltpu.make_async_copy(
                    source.at[:, pl.ds((head * 3 + group) * HEAD_DIM, HEAD_DIM)],
                    weight.at[group, :, pl.ds((part * local_heads + head) * HEAD_DIM, HEAD_DIM)],
                    load_sem.at[count],
                )
                copy.start()
                loads[group].append(copy)
                count += 1

    barrier = pltpu.get_barrier_semaphore()

    def greet(k, carry):
        pl.semaphore_signal(barrier, inc=1, device_id=(lax.rem(me + k, n), tp), device_id_type=MESH)
        return carry

    lax.fori_loop(1, n, greet, 0)
    pl.semaphore_signal(barrier, inc=1, device_id=(me, peer), device_id_type=MESH)

    @pl.when(me < 2)
    def _():
        mid_held[0] = jnp.zeros((2, rows, width), jnp.bfloat16)

    @pl.when(me < 1)
    def _():
        mid_held[1] = jnp.zeros((2, rows, width), jnp.bfloat16)
        near_held[...] = jnp.zeros((NEAR_WINDOW, 2 * width), jnp.bfloat16)

    def project(group, first, extent):
        return jnp.dot(
            tok[...], weight[group, :, first : first + extent], preferred_element_type=jnp.float32
        ).astype(jnp.bfloat16)

    def at_rows(index):
        return pl.ds(pl.multiple_of(index * chunk, chunk), chunk)

    swap = swap_matrix(rows, n)
    tok_load.wait()
    for copy in loads[2]:
        copy.wait()
    for part in range(3):
        block = project(2, part * width, width)
        far_send[:, part * width : (part + 1) * width] = jnp.dot(
            swap, block, preferred_element_type=jnp.float32
        ).astype(jnp.bfloat16)
    far_held[at_rows(me), :] = far_send[at_rows(me), :]

    def exchange(source, target, ssem, rsem, k, outgoing):
        to = lax.rem(me + k, n)
        come = lax.rem(me + n - k, n)
        return pltpu.make_async_remote_copy(
            src_ref=source.at[at_rows(to)],
            dst_ref=target.at[at_rows(me if outgoing else come)],
            send_sem=ssem.at[k],
            recv_sem=rsem.at[k],
            device_id=(to, tp),
            device_id_type=MESH,
        )

    def far_copy(k, outgoing):
        return exchange(far_send, far_held, far_ssem, far_rsem, k, outgoing)

    def back_copy(k, outgoing):
        return exchange(back_send, back_held, back_ssem, back_rsem, k, outgoing)

    def each(action):
        def step(k, carry):
            action(k)
            return carry

        lax.fori_loop(1, n, step, 0)

    pl.semaphore_wait(barrier, n)
    each(lambda k: far_copy(k, True).start())

    for copy in loads[1]:
        copy.wait()
    mid_own[0] = project(1, width, width)
    mid_own[1] = project(1, 2 * width, width)

    def mid_copy(slot, hop, source, part, sem):
        return pltpu.make_async_remote_copy(
            src_ref=source,
            dst_ref=mid_held.at[slot, part],
            send_sem=mid_ssem.at[sem, part],
            recv_sem=mid_rsem.at[slot, part],
            device_id=(lax.rem(me + hop + n, n), tp),
            device_id_type=MESH,
        )

    def via_copy():
        return pltpu.make_async_remote_copy(
            src_ref=mid_own.at[1],
            dst_ref=via_held,
            send_sem=via_ssem,
            recv_sem=via_rsem,
            device_id=(lax.rem(me + -2 + n, n), tp),
            device_id_type=MESH,
        )

    def near_copy():
        return pltpu.make_async_remote_copy(
            src_ref=near_own.at[pl.ds(rows - NEAR_WINDOW, NEAR_WINDOW)],
            dst_ref=near_held,
            send_sem=near_ssem,
            recv_sem=near_rsem,
            device_id=(lax.rem(me + 1, n), tp),
            device_id_type=MESH,
        )

    even = lax.rem(me, 2) == 0
    sends_one = me + 1 < n
    sends_two = even & (me + 2 < n)
    relays = even & (me >= 1)

    crosses = (lax.rem(me, 4) >= 2) & sends_one & (me + 4 - lax.rem(me, 4) < n)
    forwards = (lax.rem(me, 4) < 2) & (me + 4 - lax.rem(me, 4) < n)
    forward_even = forwards & even
    forward_odd = forwards & jnp.logical_not(even)

    @pl.when(crosses)
    def _():
        via_copy().start()

    @pl.when(sends_two)
    def _():
        mid_copy(0, 2, mid_own.at[0], 0, 0).start()

    @pl.when(sends_one)
    def _():
        mid_copy(1, 1, mid_own.at[0], 0, 1).start()

    @pl.when(sends_two & jnp.logical_not(crosses))
    def _():
        mid_copy(0, 2, mid_own.at[1], 1, 0).start()

    own_value_one = sends_one & jnp.logical_not(crosses & jnp.logical_not(even))

    @pl.when(own_value_one)
    def _():
        mid_copy(1, 1, mid_own.at[1], 1, 1).start()

    for copy in loads[0]:
        copy.wait()
    near_own[:, :width] = project(0, width, width)
    near_own[:, width:] = project(0, 2 * width, width)

    @pl.when(sends_one)
    def _():
        near_copy().start()

    mid_query[...] = project(1, 0, width)
    near_query[...] = project(0, 0, width)

    def slope_of(head, window):
        number = tp * local_heads + head
        slope = jnp.float32(0.0)
        for index in range(HEADS):
            value = 2.0 ** (3.0 - 8.0 * (index + 1.0) / HEADS) / window
            slope = jnp.where(number == index, jnp.float32(value), slope)
        return slope

    def spacing(row_count, key_count, offset):
        row = lax.broadcasted_iota(jnp.int32, (row_count, key_count), 0)
        column = lax.broadcasted_iota(jnp.int32, (row_count, key_count), 1)
        return row + offset - column, column

    each(lambda k: far_copy(k, False).wait_recv())

    @pl.when(forwards)
    def _():
        via_copy().wait_recv()

    @pl.when(forward_even)
    def _():
        mid_copy(0, 4, via_held, 1, 3).start()

    @pl.when(forward_odd)
    def _():
        mid_copy(1, 3, via_held, 1, 3).start()

    reach = FAR_WINDOW // FAR_DILATION
    apart, column = spacing(rows, rows, 0)
    valid = (apart >= 0) & (apart <= reach)
    distance = (apart * FAR_DILATION).astype(jnp.float32)
    lane = lax.broadcasted_iota(jnp.int32, (rows, HEAD_DIM), 1)
    packed = jnp.zeros((rows, HEAD_DIM), jnp.float32)
    for head in range(local_heads):
        at = head * HEAD_DIM
        attended, log_sum = attend(
            far_held[:, at : at + HEAD_DIM],
            far_held[:, width + at : width + at + HEAD_DIM],
            far_held[:, 2 * width + at : 2 * width + at + HEAD_DIM],
            slope_of(head, FAR_WINDOW), distance, valid,
        )
        back_send[:, at : at + HEAD_DIM] = attended.astype(jnp.bfloat16)
        rest = log_sum
        for term in range(3):
            piece = rest.astype(jnp.bfloat16).astype(jnp.float32)
            packed = jnp.where(lane == 3 * head + term, piece, packed)
            rest = rest - piece
    back_send[:, width:] = packed.astype(jnp.bfloat16)
    back_held[at_rows(me), :] = back_send[at_rows(me), :]
    each(lambda k: back_copy(k, True).start())

    @pl.when(me >= 1)
    def _():
        near_copy().wait_recv()
        mid_copy(1, 1, mid_own.at[0], 0, 1).wait_recv()
        mid_copy(1, 1, mid_own.at[1], 1, 1).wait_recv()

    @pl.when(relays)
    def _():
        mid_copy(0, 1, mid_held.at[1, 0], 0, 2).start()
        mid_copy(0, 1, mid_held.at[1, 1], 1, 2).start()

    apart, column = spacing(rows, NEAR_WINDOW + rows, NEAR_WINDOW)
    valid = (apart >= 0) & (apart <= NEAR_WINDOW) & (column + me * rows >= NEAR_WINDOW)
    distance = apart.astype(jnp.float32)
    near = []
    for head in range(local_heads):
        at = head * HEAD_DIM
        key = jnp.concatenate((near_held[:, at : at + HEAD_DIM], near_own[:, at : at + HEAD_DIM]), axis=0)
        at2 = width + at
        value = jnp.concatenate((near_held[:, at2 : at2 + HEAD_DIM], near_own[:, at2 : at2 + HEAD_DIM]), axis=0)
        near.append(attend(near_query[:, at : at + HEAD_DIM], key, value, slope_of(head, NEAR_WINDOW), distance, valid))

    @pl.when(me >= 2)
    def _():
        mid_copy(0, 2, mid_own.at[0], 0, 0).wait_recv()
        mid_copy(0, 2, mid_own.at[1], 1, 0).wait_recv()

    apart, column = spacing(rows, MIDDLE_WINDOW + rows, MIDDLE_WINDOW)
    valid = (apart >= 0) & (apart <= MIDDLE_WINDOW) & ((apart & (MIDDLE_DILATION - 1)) == 0)
    valid = valid & (column + me * rows >= MIDDLE_WINDOW)
    distance = apart.astype(jnp.float32)
    middle = []
    for head in range(local_heads):
        at = head * HEAD_DIM
        key = jnp.concatenate([x[:, at : at + HEAD_DIM] for x in (mid_held[0, 0], mid_held[1, 0], mid_own[0])], axis=0)
        value = jnp.concatenate([x[:, at : at + HEAD_DIM] for x in (mid_held[0, 1], mid_held[1, 1], mid_own[1])], axis=0)
        middle.append(attend(mid_query[:, at : at + HEAD_DIM], key, value, slope_of(head, MIDDLE_WINDOW), distance, valid))

    each(lambda k: back_copy(k, False).wait_recv())
    far = jnp.dot(swap, back_held[...], preferred_element_type=jnp.float32)
    parts = far[:, width:]
    totals = jnp.zeros((rows, HEAD_DIM), jnp.float32)
    for head in range(local_heads):
        at = head * HEAD_DIM
        far_log = jnp.sum(
            jnp.where((lane >= 3 * head) & (lane < 3 * head + 3), parts, 0.0), axis=-1, keepdims=True
        )
        near_log, middle_log = near[head][1], middle[head][1]
        highest = jnp.maximum(jnp.maximum(near_log, middle_log), far_log)
        total = highest + jnp.log(
            jnp.exp(near_log - highest) + jnp.exp(middle_log - highest) + jnp.exp(far_log - highest)
        )
        merged = near[head][0] * jnp.exp(near_log - total)
        merged = merged + middle[head][0] * jnp.exp(middle_log - total)
        merged = merged + far[:, at : at + HEAD_DIM] * jnp.exp(far_log - total)
        merged_own[:, at : at + HEAD_DIM] = merged.astype(jnp.bfloat16)
        totals = jnp.where(lane == head, total, totals)

    swap_merged = pltpu.make_async_remote_copy(
        src_ref=merged_own,
        dst_ref=merged_held,
        send_sem=merged_ssem,
        recv_sem=merged_rsem,
        device_id=(me, peer),
        device_id_type=MESH,
    )
    swap_merged.start()
    totals_ref[...] = totals
    both_ref[tp] = merged_own[...]
    swap_merged.wait_recv()
    both_ref[peer] = merged_held[...]

    swap_merged.wait_send()
    each(lambda k: far_copy(k, True).wait_send())
    each(lambda k: back_copy(k, True).wait_send())

    @pl.when(crosses)
    def _():
        via_copy().wait_send()

    @pl.when(sends_two)
    def _():
        mid_copy(0, 2, mid_own.at[0], 0, 0).wait_send()

    @pl.when(sends_two & jnp.logical_not(crosses))
    def _():
        mid_copy(0, 2, mid_own.at[1], 1, 0).wait_send()

    @pl.when(sends_one)
    def _():
        mid_copy(1, 1, mid_own.at[0], 0, 1).wait_send()
        near_copy().wait_send()

    @pl.when(own_value_one)
    def _():
        mid_copy(1, 1, mid_own.at[1], 1, 1).wait_send()

    @pl.when(forward_even)
    def _():
        mid_copy(0, 4, via_held, 1, 3).wait_send()

    @pl.when(forward_odd)
    def _():
        mid_copy(1, 3, via_held, 1, 3).wait_send()

    @pl.when(relays)
    def _():
        mid_copy(0, 1, mid_held.at[1, 0], 0, 2).wait_send()
        mid_copy(0, 1, mid_held.at[1, 1], 1, 2).wait_send()


def mix(both_ref, totals_ref, wo_ref, mixed_ref, log_ref):
    width = both_ref.shape[2]
    product = jnp.dot(both_ref[0], wo_ref[:width], preferred_element_type=jnp.float32)
    product = product + jnp.dot(both_ref[1], wo_ref[width:], preferred_element_type=jnp.float32)
    mixed_ref[...] = product.astype(jnp.bfloat16)
    log_ref[...] = jnp.transpose(totals_ref[...])[: log_ref.shape[0]]


def fused(n, n_tp, tokens, query_weight, key_weight, value_weight, out_weight):
    rows, depth = tokens.shape
    columns = query_weight.shape[1]
    local_heads = columns // (3 * HEAD_DIM)
    width = local_heads * HEAD_DIM
    dma = pltpu.SemaphoreType.DMA
    half = jnp.bfloat16
    both, totals = pl.pallas_call(
        functools.partial(kernel, n, n_tp, local_heads),
        out_shape=(
            jax.ShapeDtypeStruct((n_tp, rows, width), half),
            jax.ShapeDtypeStruct((rows, HEAD_DIM), jnp.float32),
        ),
        in_specs=[pl.BlockSpec(memory_space=pl.ANY)] * 4,
        out_specs=(pl.BlockSpec(memory_space=pltpu.VMEM), pl.BlockSpec(memory_space=pltpu.VMEM)),
        scratch_shapes=[
            pltpu.VMEM((rows, depth), half),
            pltpu.VMEM((3, depth, columns), half),
            pltpu.VMEM((rows, columns), half),
            pltpu.VMEM((rows, columns), half),
            pltpu.VMEM((rows, width + HEAD_DIM), half),
            pltpu.VMEM((rows, width + HEAD_DIM), half),
            pltpu.VMEM((rows, width), half),
            pltpu.VMEM((2, rows, width), half),
            pltpu.VMEM((2, 2, rows, width), half),
            pltpu.VMEM((rows, width), half),
            pltpu.VMEM((rows, width), half),
            pltpu.VMEM((rows, 2 * width), half),
            pltpu.VMEM((NEAR_WINDOW, 2 * width), half),
            pltpu.VMEM((rows, width), half),
            pltpu.VMEM((rows, width), half),
            dma((1 + 9 * local_heads,)),
            dma((n,)), dma((n,)), dma((n,)), dma((n,)),
            dma((4, 2)), dma((2, 2)), dma(()), dma(()), dma(()), dma(()), dma(()), dma(()),
        ],
        compiler_params=pltpu.CompilerParams(
            collective_id=0, has_side_effects=True, vmem_limit_bytes=63900 * 1024
        ),
    )(tokens, query_weight, key_weight, value_weight)
    whole = pl.BlockSpec(memory_space=pltpu.VMEM)
    return pl.pallas_call(
        mix,
        out_shape=(
            jax.ShapeDtypeStruct((rows, out_weight.shape[1]), half),
            jax.ShapeDtypeStruct((local_heads, rows), jnp.float32),
        ),
        in_specs=[whole] * 3,
        out_specs=(whole, whole),
        compiler_params=pltpu.CompilerParams(vmem_limit_bytes=16000 * 1024),
    )(both, totals, out_weight)


def solution(mesh):
    n, n_tp = mesh.shape["sp"], mesh.shape["tp"]
    if n == FAR_DILATION and n_tp == 2:
        body = functools.partial(fused, n, n_tp)
    else:
        body = local
    return jax.shard_map(
        body,
        mesh=mesh,
        in_specs=(P("sp", None), P(None, "tp"), P(None, "tp"), P(None, "tp"), P(None, "tp")),
        out_specs=(P("sp", "tp"), P("tp", "sp")),
        check_vma=False,
    )
```

profile of v0, /device:TPU:17, one launch (start us, length us, event | category | flops | bytes accessed | tf_op | source)
XLA Modules:
  0.0 36.6 jit_solution(13935413561061916259)
XLA Ops:
  0.6 0.0 copy-start
  0.6 32.8 %shard_map.68 = (bf16[2,256,256]{2,1,0:T(8,128)(2,1)}, f32[256,128]{1,0:T(8,128)}) custom-call(bf16[256,2048]{1,0:T(8,128)(2,1)} %tok_hbm.1, bf16[2048,768]{1,0:T(8,128)(2,1)} %wq_hbm.1, bf16[2048,768]{1,0:T(8,128)(2,1)} %wk_hbm.1, bf16[2048,768]{1,0:T(8,128)(2,1)} %wv_hbm.1), custom_call_target="tpu_custom_call" | custom-call | tf_op jit(solution)/shard_map/pallas_call | solution.py:520
  33.5 0.0 copy-done
  33.5 0.0 copy-start.1
  33.5 0.9 %copy-done.1 = bf16[2,256,256]{2,1,0:T(8,128)(2,1)S(1)} copy-done((bf16[2,256,256]{2,1,0:T(8,128)(2,1)S(1)}, bf16[2,256,256]{2,1,0:T(8,128)(2,1)}, u32[]{:S(2)}) %copy-start.1) | copy-done | bytes 262168
  34.4 0.0 copy-start.2
  34.4 0.9 %copy-done.2 = f32[256,128]{1,0:T(8,128)S(1)} copy-done((f32[256,128]{1,0:T(8,128)S(1)}, f32[256,128]{1,0:T(8,128)}, u32[]{:S(2)}) %copy-start.2) | copy-done | bytes 131096
  35.3 1.3 %shard_map.69 = (bf16[256,1024]{1,0:T(8,128)(2,1)}, f32[2,256]{1,0:T(2,128)}) custom-call(bf16[2,256,256]{2,1,0:T(8,128)(2,1)S(1)} %copy-done.1, f32[256,128]{1,0:T(8,128)S(1)} %copy-done.2, bf16[512,1024]{1,0:T(8,128)(2,1)S(1)} %copy-done), custom_call_target="tpu_custom_call" | custom-call | tf_op jit(solution)/shard_map/pallas_call | solution.py:553
Async XLA Ops:
  0.6 32.9 %copy-start = (bf16[512,1024]{1,0:T(8,128)(2,1)S(1)}, bf16[512,1024]{1,0:T(8,128)(2,1)}, u32[]{:S(2)}) copy-start(bf16[512,1024]{1,0:T(8,128)(2,1)} %wo_ref.1) | copy-start | bytes 3145732
  33.5 1.0 %copy-start.1 = (bf16[2,256,256]{2,1,0:T(8,128)(2,1)S(1)}, bf16[2,256,256]{2,1,0:T(8,128)(2,1)}, u32[]{:S(2)}) copy-start(bf16[2,256,256]{2,1,0:T(8,128)(2,1)} %get-tuple-element.4.both_ref) | copy-start | bytes 786436
  34.4 0.9 %copy-start.2 = (f32[256,128]{1,0:T(8,128)S(1)}, f32[256,128]{1,0:T(8,128)}, u32[]{:S(2)}) copy-start(f32[256,128]{1,0:T(8,128)} %get-tuple-element.5.totals_ref) | copy-start | bytes 393220
where the time goes:
time: 36.8 us; the launch traced here: 36.6 us
  Pallas kernels  34.1 us (93%)
  local copies, waits for them, and re-layouts  1.85 us (5%)
  between operations  0.66 us (2%)
    pallas_call x1, Pallas kernels, fused(): pl.pallas_call(functools.partial(kernel, n, n_tp, local_heads), out_shape...  32.8 us
    unnamed x6, local copies, waits for them, and re-layouts  1.85 us
    pallas_call x1, Pallas kernels, fused(): pl.pallas_call(mix, out_shape=(jax.ShapeDtypeStruct((rows, out_weight.sha...  1.26 us

commit v1 on v0

--- a/solution.py
+++ b/solution.py
@@ -224,9 +224,9 @@
 
     swap = swap_matrix(rows, n)
     tok_load.wait()
-    for copy in loads[2]:
-        copy.wait()
     for part in range(3):
+        for copy in loads[2][part * local_heads : (part + 1) * local_heads]:
+            copy.wait()
         block = project(2, part * width, width)
         far_send[:, part * width : (part + 1) * width] = jnp.dot(
             swap, block, preferred_element_type=jnp.float32
@@ -546,7 +546,7 @@
             dma((4, 2)), dma((2, 2)), dma(()), dma(()), dma(()), dma(()), dma(()), dma(()),
         ],
         compiler_params=pltpu.CompilerParams(
-            collective_id=0, has_side_effects=True, vmem_limit_bytes=63900 * 1024
+            collective_id=0, has_side_effects=True, vmem_limit_bytes=54000 * 1024
         ),
     )(tokens, query_weight, key_weight, value_weight)
     whole = pl.BlockSpec(memory_space=pltpu.VMEM)

time: 36.8 us -> 33.7 us (0.916)
  local copies, waits for them, and re-layouts: 1.85 us -> 0.01 us
  Pallas kernels: 34.1 us -> 32.9 us
    unnamed x6 -> x2, local copies, waits for them, and re-layouts: 1.85 us -> 0.01 us
    pallas_call x1, Pallas kernels: 32.8 us -> 31.7 us  [fused(): pl.pallas_call(functools.partial(kernel, n, n_tp, local_heads), out_shape...]
where the time goes in v1:
time: 33.7 us; the launch traced here: 33.6 us
  Pallas kernels  32.9 us (98%)
  between operations  0.65 us (2%)
    pallas_call x1, Pallas kernels, fused(): pl.pallas_call(functools.partial(kernel, n, n_tp, local_heads), out_shape...  31.7 us
    pallas_call x1, Pallas kernels, fused(): pl.pallas_call(mix, out_shape=(jax.ShapeDtypeStruct((rows, out_weight.sha...  1.24 us

profile of v1, /device:TPU:17, one launch (start us, length us, event | category | flops | bytes accessed | tf_op | source)
XLA Modules:
  0.0 33.6 jit_solution(6030548355033686006)
XLA Ops:
  0.6 0.0 copy-start
  0.6 31.7 %shard_map.68 = (bf16[2,256,256]{2,1,0:T(8,128)(2,1)S(1)}, f32[256,128]{1,0:T(8,128)S(1)}) custom-call(bf16[256,2048]{1,0:T(8,128)(2,1)} %tok_hbm.1, bf16[2048,768]{1,0:T(8,128)(2,1)} %wq_hbm.1, bf16[2048,768]{1,0:T(8,128)(2,1)} %wk_hbm.1, bf16[2048,768]{1,0:T(8,128)(2,1)} %wv_hbm.1), custom_call_target="tpu_custom_call" | custom-call | tf_op jit(solution)/shard_map/pallas_call | solution.py:520
  32.3 0.0 copy-done
  32.3 1.2 %shard_map.69 = (bf16[256,1024]{1,0:T(8,128)(2,1)}, f32[2,256]{1,0:T(2,128)}) custom-call(bf16[2,256,256]{2,1,0:T(8,128)(2,1)S(1)} %get-tuple-element.4.both_ref, f32[256,128]{1,0:T(8,128)S(1)} %get-tuple-element.5.totals_ref, bf16[512,1024]{1,0:T(8,128)(2,1)S(1)} %copy-done), custom_call_target="tpu_custom_call" | custom-call | tf_op jit(solution)/shard_map/pallas_call | solution.py:553
Async XLA Ops:
  0.6 31.7 %copy-start = (bf16[512,1024]{1,0:T(8,128)(2,1)S(1)}, bf16[512,1024]{1,0:T(8,128)(2,1)}, u32[]{:S(2)}) copy-start(bf16[512,1024]{1,0:T(8,128)(2,1)} %wo_ref.1) | copy-start | bytes 3145732
